TPU v7x, 32 devices: a whole 2x2x4 slice. The times are simulated.
32 devices in a mesh: sp: 16 (over z, y, x), tp: 2 (over core).
Axes of the slice: x: 2, y: 2, z: 4, core: 2. Of those that a mesh axis runs over, the one named last changes fastest.
Arguments:
- queries: bfloat16 [3072, 1024], P('sp', 'tp'), may hold values from -6 to 6
- keys: bfloat16 [3072, 512], P('sp', 'tp'), may hold values from -6 to 6
- values: bfloat16 [3072, 512], P('sp', 'tp'), may hold values from -6 to 6
- query_gain: float32 [16, 64], P('tp'), may hold values from 1.4 to 7.5
- key_gain: float32 [8, 64], P('tp'), may hold values from 1.4 to 7.5
- out_weight: bfloat16 [1024, 2048], P('tp'), may hold values from -0.375 to 0.375
- residual: bfloat16 [3072, 2048], P('sp'), may hold values from -170 to 170
- norm_gain: float32 [2048], replicated, may hold values from 0.1 to 1.9
- gate_weight: bfloat16 [2048, 5632], P('sp', 'tp'), may hold values from -0.125 to 0.125
- up_weight: bfloat16 [2048, 5632], P('sp', 'tp'), may hold values from -0.125 to 0.125
- down_weight: bfloat16 [5632, 2048], P('tp', 'sp'), may hold values from -0.15625 to 0.15625
Outputs:
- mixed: bfloat16 [3072, 2048], P('sp')
All inputs are finite; a program needn't handle non-finite values.
Results may differ from a plain program's by a relative error of at most 0.017.
Values may be sent and summed in bfloat16 or wider, within the bound.
A program may use at most 128 MiB of HBM per device.

v0:
```python
import jax
import jax.numpy as jnp
from jax import lax
from jax.sharding import PartitionSpec as P

GRID_W = 64
epsilon = 1e-06
rope_base = 10000.0
block_keys = 2048


def rotate_pairs(entries, places):
    half = entries.shape[-1] // 2
    frequency = rope_base ** (-jnp.arange(half, dtype=jnp.float32) / half)
    angle = places.astype(jnp.float32)[:, None, None] * frequency[None, None, :]
    cosine = jnp.cos(angle)
    sine = jnp.sin(angle)
    first = entries[..., :half]
    second = entries[..., half:]
    return jnp.concatenate(
        [first * cosine - second * sine, first * sine + second * cosine], axis=-1
    )


def grid_rotate(entries, grid_rows, grid_cols):
    half = entries.shape[-1] // 2
    return jnp.concatenate(
        [
            rotate_pairs(entries[..., :half], grid_rows),
            rotate_pairs(entries[..., half:], grid_cols),
        ],
        axis=-1,
    )


def head_norm(entries, gains):
    factor = lax.rsqrt(jnp.mean(entries * entries, axis=-1, keepdims=True) + epsilon)
    return entries * factor * gains[None]


def row_norm(mid, norm_gain):
    wide = mid.astype(jnp.float32)
    return (
        wide * lax.rsqrt(jnp.mean(wide * wide, axis=-1, keepdims=True) + epsilon) * norm_gain
    ).astype(jnp.bfloat16)


def block_span(length):
    if length <= block_keys:
        return length
    span = block_keys
    while length % span != 0:
        span = span - 1
    return span


def body(
    queries,
    keys,
    values,
    query_gain,
    key_gain,
    out_weight,
    residual,
    norm_gain,
    gate_weight,
    up_weight,
    down_weight,
):
    own = queries.shape[0]
    heads = query_gain.shape[0]
    key_heads = key_gain.shape[0]
    head_size = query_gain.shape[1]
    group = heads // key_heads
    gate_full, up_full, down_full = (
        lax.all_gather(gate_weight, "sp", axis=0, tiled=True),
        lax.all_gather(up_weight, "sp", axis=0, tiled=True),
        lax.all_gather(down_weight, "sp", axis=1, tiled=True),
    )
    places = lax.axis_index("sp") * own + jnp.arange(own, dtype=jnp.int32)
    grid_rows = places // GRID_W
    grid_cols = places % GRID_W
    query_turned = grid_rotate(
        head_norm(queries.astype(jnp.float32).reshape(own, heads, head_size), query_gain),
        grid_rows,
        grid_cols,
    ).astype(jnp.bfloat16)
    query_groups = query_turned.reshape(own, key_heads, group, head_size)
    key_turned = (
        grid_rotate(
            head_norm(keys.astype(jnp.float32).reshape(own, key_heads, head_size), key_gain),
            grid_rows,
            grid_cols,
        )
        .astype(jnp.bfloat16)
        .reshape(own, key_heads * head_size)
    )
    scale = head_size ** (-0.5)

    def absorb(carry, key_block, value_block):
        top, total, summed = carry
        key_block = key_block.reshape(-1, key_heads, head_size)
        value_block = value_block.reshape(-1, key_heads, head_size)
        score = (
            jnp.einsum(
                "qgrd,kgd->qgrk", query_groups, key_block, preferred_element_type=jnp.float32
            )
            * scale
        )
        new_top = jnp.maximum(top, jnp.max(score, axis=-1))
        weight = jnp.exp(score - new_top[..., None])
        shrink = jnp.exp(top - new_top)
        total = total * shrink + jnp.sum(weight, axis=-1)
        summed = summed * shrink[..., None] + jnp.einsum(
            "qgrk,kgd->qgrd",
            weight.astype(jnp.bfloat16),
            value_block,
            preferred_element_type=jnp.float32,
        )
        return (new_top, total, summed)

    def fold_keys(carry, pieces):
        length = pieces[0].shape[0]
        span = block_span(length)
        if span == length:
            return absorb(carry, pieces[0], pieces[1])
        width = pieces[0].shape[1]
        key_blocks = pieces[0].reshape(length // span, span, width)
        value_blocks = pieces[1].reshape(length // span, span, width)

        def scan_step(inner, blocks):
            return (absorb(inner, blocks[0], blocks[1]), None)

        result, unused = lax.scan(scan_step, carry, (key_blocks, value_blocks))
        return result

    start_state = (
        jnp.full((own, key_heads, group), -jnp.inf, jnp.float32),
        jnp.zeros((own, key_heads, group), jnp.float32),
        jnp.zeros((own, key_heads, group, head_size), jnp.float32),
    )
    top, total, summed = fold_keys(
        start_state,
        (
            lax.all_gather(key_turned, "sp", axis=0, tiled=True),
            lax.all_gather(values, "sp", axis=0, tiled=True),
        ),
    )
    attended = (summed / total[..., None]).reshape(own, heads * head_size).astype(jnp.bfloat16)
    part_rows = own // lax.axis_size("tp")
    branch = lax.psum_scatter(
        jnp.dot(
            lax.slice_in_dim(attended, 0, lax.axis_size("tp") * part_rows, axis=0),
            out_weight,
            preferred_element_type=jnp.float32,
        ).astype(jnp.bfloat16),
        "tp",
        scatter_dimension=0,
        tiled=True,
    ).astype(jnp.float32)
    own_rows = lax.dynamic_slice_in_dim(residual, lax.axis_index("tp") * part_rows, part_rows, 0)
    mid = (own_rows.astype(jnp.float32) + branch).astype(jnp.bfloat16)
    normed_all = lax.all_gather(row_norm(mid, norm_gain), "tp", axis=0, tiled=True)
    gate = jnp.dot(normed_all, gate_full, preferred_element_type=jnp.float32)
    up_value = jnp.dot(normed_all, up_full, preferred_element_type=jnp.float32)
    hidden = (jax.nn.silu(gate) * up_value).astype(jnp.bfloat16)
    terms = jnp.dot(hidden, down_full, preferred_element_type=jnp.float32)
    ffn = lax.psum_scatter(
        terms.astype(jnp.bfloat16), "tp", scatter_dimension=0, tiled=True
    ).astype(jnp.float32)
    finished = (mid.astype(jnp.float32) + ffn).astype(jnp.bfloat16)
    return lax.all_gather(finished, "tp", axis=0, tiled=True)


def solution(mesh):
    in_specs = (
        P("sp", "tp"),
        P("sp", "tp"),
        P("sp", "tp"),
        P("tp", None),
        P("tp", None),
        P("tp", None),
        P("sp", None),
        P(),
        P("sp", "tp"),
        P("sp", "tp"),
        P("tp", "sp"),
    )
    out_specs = P("sp", None)
    return jax.shard_map(body, mesh=mesh, in_specs=in_specs, out_specs=out_specs, check_vma=False)
```

profile of v0, /device:TPU:0, one launch (start us, length us, event | category | flops | bytes accessed | tf_op | source)
XLA Modules:
  0.0 684.2 jit_solution(15495165526293549305)
XLA Ops:
  6.6 1.1 copy.22
  7.8 0.8 fusion.22
  10.4 1.1 copy.24
  11.6 0.8 fusion.20
  13.3 57.5 %all-gather.6.cloned.1.call-done = bf16[3072,256]{1,0:T(8,128)(2,1)} async-done(((bf16[192,256]{1,0:T(8,128)(2,1)}), bf16[3072,256]{1,0:T(8,128)(2,1)}) %all-gather.6.cloned.1.call-update) | async-done | bytes 1572880 | tf_op jit(solution)/shard_map/all_gather | solution.py:145
  70.8 59.5 %all-gather.8.cloned.1.call-done = bf16[3072,256]{1,0:T(8,128)(2,1)} async-done(((bf16[192,256]{1,0:T(8,128)(2,1)}), bf16[3072,256]{1,0:T(8,128)(2,1)}) %all-gather.8.cloned.1.call-update) | async-done | bytes 1572880 | tf_op jit(solution)/shard_map/all_gather | solution.py:146
  130.3 43.6 %while.15 = (s32[]{:T(128)}, f32[192,4,2]{0,2,1:T(2,128)S(1)}, f32[192,4,2]{0,2,1:T(2,128)S(1)}, f32[192,4,2,64]{0,3,2,1:T(8,128)S(1)}, bf16[2,1536,256]{2,1,0:T...) while((s32[]{:T(128)}, f32[192,4,2]{0,2,1:T(2,128)S(1)}, ...), condition=%wide.region_5.6_spmd.clone, body=%wide.region_2.5_spmd.clone.sunk | while | flops 623156736 | bytes 37257324 | solution.py:134
  130.3 2.6 constant_dynamic-slice_fusion.3
  132.9 1.4 copy.33
  134.3 6.0 bitcast_reduce_fusion.2
  140.4 5.4 fusion.51
  145.8 1.4 copy.34
  147.2 4.8 fusion.53
  152.1 2.6 constant_dynamic-slice_fusion.3
  154.7 1.4 copy.33
  156.1 6.0 bitcast_reduce_fusion.2
  162.1 5.4 fusion.51
  167.6 1.4 copy.34
  169.0 4.8 fusion.53
  173.9 1.5 convolution_convert_fusion.1
  177.2 5.2 reduce-scatter.3.cloned.1.call-done
  182.5 1.4 fusion.15
  184.0 2.5 all_gather.23
  186.6 141.1 %all-gather.10.cloned.1.call-done = bf16[2048,2816]{1,0:T(8,128)(2,1)} async-done(((bf16[128,2816]{1,0:T(8,128)(2,1)}), bf16[2048,2816]{1,0:T(8,128)(2,1)}) %all-gather.10.cloned.1.call-update) | async-done | bytes 11534352 | tf_op jit(solution)/shard_map/all_gather | solution.py:76
  327.6 8.0 %fusion.27 = f32[192,2816]{1,0:T(8,128)} fusion(bf16[192,2048]{1,0:T(8,128)(2,1)S(1)} %all_gather.23, bf16[2048,2816]{1,0:T(8,128)(2,1)} %all-gather.10.cloned.1.call-done), kind=kOutput, calls=%fused_computation.67 | convolution fusion | flops 2214592512 | bytes 14483456 | tf_op jit(solution)/shard_map/dot_general | solution.py:164
  335.7 134.2 %all-gather.12.cloned.1.call-done = bf16[2048,2816]{1,0:T(8,128)(2,1)} async-done(((bf16[128,2816]{1,0:T(8,128)(2,1)}), bf16[2048,2816]{1,0:T(8,128)(2,1)}) %all-gather.12.cloned.1.call-update) | async-done | bytes 11534352 | tf_op jit(solution)/shard_map/all_gather | solution.py:77
  469.9 182.8 %all-gather.14.cloned.1.call-done = bf16[2816,2048]{1,0:T(8,128)(2,1)} async-done(((bf16[2816,128]{1,0:T(8,128)(2,1)}), bf16[2816,2048]{1,0:T(8,128)(2,1)}) %all-gather.14.cloned.1.call-update) | async-done | bytes 11534352 | tf_op jit(solution)/shard_map/all_gather | solution.py:78
  652.7 13.8 %convolution_convert_fusion = bf16[192,2048]{1,0:T(8,128)(2,1)} fusion(bf16[2816,2048]{1,0:T(8,128)(2,1)} %all-gather.14.cloned.1.call-done, bf16[192,2048]{1,0:T(8,128)(2,1)S(1)} %all_gather.23, bf16[2048,2816]{1,0:T(8,128)(2,1)} %all-gather.12.cloned.1.call-done, f32[192,2816]{1,0:T(8,128)} %fusion.27), kind=kOutput, calls=%fused_computation.19 | convolution fusion | flops 4432822272 | bytes 26804224 | tf_op jit(solution)/shard_map/dot_general | solution.py:167
  666.5 6.5 reduce-scatter.5.cloned.1.call-done
  673.0 1.1 fusion.18
  674.1 2.4 all_gather.27
  676.5 0.9 copy.48
  (42 shorter events, 4.9 us)
Async XLA Ops:
  6.5 167.4 %copy-start = (bf16[512,2048]{1,0:T(8,128)(2,1)S(1)}, bf16[512,2048]{1,0:T(8,128)(2,1)}, u32[]{:S(2)}) copy-start(bf16[512,2048]{1,0:T(8,128)(2,1)} %param.18) | copy-start | bytes 6291460
  6.5 64.3 %all-gather.6.cloned.1.call-start = ((), (), s32[]{:S(2)}) async-start(), calls=%async_computation.2 | async-start | bytes 1671168 | tf_op jit(solution)/shard_map/all_gather | solution.py:145
  9.6 120.7 %all-gather.8.cloned.1.call-start = ((), (), s32[]{:S(2)}) async-start(), calls=%async_computation.3 | async-start | bytes 1671168 | tf_op jit(solution)/shard_map/all_gather | solution.py:146
  10.4 172.1 %reduce-scatter.3.cloned.1.call-start = ((), (), s32[]{:S(2)}) async-start(), calls=%async_computation.4 | async-start | bytes 1179648 | tf_op jit(solution)/shard_map/reduce_scatter | solution.py:151
  130.3 53.6 %copy-start.1 = (f32[2048]{0:T(1024)S(1)}, f32[2048]{0:T(1024)}, u32[]{:S(2)}) copy-start(f32[2048]{0:T(1024)} %param.20) | copy-start | bytes 24580
  175.4 152.2 %all-gather.10.cloned.1.call-start = ((), (), s32[]{:S(2)}) async-start(), calls=%async_computation.5 | async-start | bytes 12255232 | tf_op jit(solution)/shard_map/all_gather | solution.py:76
  176.0 293.9 %all-gather.12.cloned.1.call-start = ((), (), s32[]{:S(2)}) async-start(), calls=%async_computation.6 | async-start | bytes 12255232 | tf_op jit(solution)/shard_map/all_gather | solution.py:77
  176.6 476.1 %all-gather.14.cloned.1.call-start = ((), (), s32[]{:S(2)}) async-start(), calls=%async_computation.7 | async-start | bytes 12255232 | tf_op jit(solution)/shard_map/all_gather | solution.py:78
  177.2 495.9 %reduce-scatter.5.cloned.1.call-start = ((), (), s32[]{:S(2)}) async-start(), calls=%async_computation.8 | async-start | bytes 1179648 | tf_op jit(solution)/shard_map/reduce_scatter | solution.py:168
Sparse Core Ops, SparseCore 0:
  10.1 60.6 all-gather.5
  73.6 56.6 all-gather.7
  175.6 6.8 reduce-scatter.2
  185.1 142.5 all-gather.9
  330.2 139.5 all-gather.11
  472.4 180.2 all-gather.13
  666.7 6.3 reduce-scatter.4
where the time goes:
time: 685 us; the launch traced here: 684 us
  waiting for transfers between devices  589 us (86%)
  matrix products  45.1 us (7%)
  other arithmetic  16.4 us (2%)
  local copies, waits for them, and re-layouts  14.7 us (2%)
  between operations  13.7 us (2%)
    all_gather x1, waiting for transfers between devices, body(): lax.all_gather(down_weight, 'sp', axis=1, tiled=True)  183 us
    all_gather x1, waiting for transfers between devices, body(): lax.all_gather(gate_weight, 'sp', axis=0, tiled=True)  141 us
    all_gather x1, waiting for transfers between devices, body(): lax.all_gather(up_weight, 'sp', axis=0, tiled=True)  134 us
    all_gather x1, waiting for transfers between devices, body(): lax.all_gather(values, 'sp', axis=0, tiled=True)  59.5 us
    all_gather x1, waiting for transfers between devices, body(): lax.all_gather(key_turned, 'sp', axis=0, tiled=True)  57.5 us
    dot_general x1, matrix products, body(): terms = jnp.dot(hidden, down_full, preferred_element_type=jnp.float32)  13.8 us
  transfers between devices with their start and end apart: 7, of which 7 were waited for; matrix products, arithmetic and copies ran while one was open for 2% of the time, Pallas kernels for 0%

commit v1 on v0

--- a/solution.py
+++ b/solution.py
@@ -2,6 +2,7 @@
 import jax.numpy as jnp
 from jax import lax
 from jax.sharding import PartitionSpec as P
+from jax.lax import all_to_all, axis_size
 
 GRID_W = 64
 epsilon = 1e-06
@@ -75,7 +76,7 @@
     gate_full, up_full, down_full = (
         lax.all_gather(gate_weight, "sp", axis=0, tiled=True),
         lax.all_gather(up_weight, "sp", axis=0, tiled=True),
-        lax.all_gather(down_weight, "sp", axis=1, tiled=True),
+        jnp.concatenate(all_to_all(jnp.stack(axis_size("sp") * [down_weight], 0), "sp", 0, 0), 1),
     )
     places = lax.axis_index("sp") * own + jnp.arange(own, dtype=jnp.int32)
     grid_rows = places // GRID_W

time: 685 us -> 714 us (1.042)
  waiting for transfers between devices: 589 us -> 605 us
    all_gather x1, waiting for transfers between devices: 141 us -> 339 us  [body(): lax.all_gather(gate_weight, 'sp', axis=0, tiled=True)]
    all_gather x1 -> x0, waiting for transfers between devices: 183 us -> none  [body(): lax.all_gather(down_weight, 'sp', axis=1, tiled=True)]
  transfers between devices with their start and end apart: 7 -> 7, of which waited for: 7 -> 5; matrix products, arithmetic and copies ran while one was open for 2% -> 3% of each run, Pallas kernels for 0% -> 0%
where the time goes in v1:
time: 714 us; the launch traced here: 713 us
  waiting for transfers between devices  605 us (85%)
  matrix products  46.5 us (7%)
  local copies, waits for them, and re-layouts  21.5 us (3%)
  other arithmetic  16.3 us (2%)
  between operations  13.7 us (2%)
    all_gather x1, waiting for transfers between devices, body(): lax.all_gather(gate_weight, 'sp', axis=0, tiled=True)  339 us
    all_gather x1, waiting for transfers between devices, body(): lax.all_gather(up_weight, 'sp', axis=0, tiled=True)  141 us
    all_gather x1, waiting for transfers between devices, body(): lax.all_gather(values, 'sp', axis=0, tiled=True)  59.5 us
    all_gather x1, waiting for transfers between devices, body(): lax.all_gather(key_turned, 'sp', axis=0, tiled=True)  57.5 us
    dot_general x1, matrix products, body(): terms = jnp.dot(hidden, down_full, preferred_element_type=jnp.float32)  15.2 us
  transfers between devices with their start and end apart: 7, of which 5 were waited for; matrix products, arithmetic and copies ran while one was open for 3% of the time, Pallas kernels for 0%

profile of v1, /device:TPU:0, one launch (start us, length us, event | category | flops | bytes accessed | tf_op | source)
XLA Modules:
  0.0 712.9 jit_solution(11170191835093642015)
XLA Ops:
  6.6 1.1 copy.23
  10.4 1.1 copy.25
  11.6 0.8 fusion.20
  13.3 57.5 %all-gather.5.cloned.1.call-done = bf16[3072,256]{1,0:T(8,128)(2,1)} async-done(((bf16[192,256]{1,0:T(8,128)(2,1)}), bf16[3072,256]{1,0:T(8,128)(2,1)}) %all-gather.5.cloned.1.call-update) | async-done | bytes 1572880 | tf_op jit(solution)/shard_map/all_gather | solution.py:146
  70.8 59.5 %all-gather.7.cloned.1.call-done = bf16[3072,256]{1,0:T(8,128)(2,1)} async-done(((bf16[192,256]{1,0:T(8,128)(2,1)}), bf16[3072,256]{1,0:T(8,128)(2,1)}) %all-gather.7.cloned.1.call-update) | async-done | bytes 1572880 | tf_op jit(solution)/shard_map/all_gather | solution.py:147
  130.3 43.5 %while.15 = (s32[]{:T(128)}, f32[192,4,2]{0,2,1:T(2,128)S(1)}, f32[192,4,2]{0,2,1:T(2,128)S(1)}, f32[192,4,2,64]{0,3,2,1:T(8,128)S(1)}, bf16[2,1536,256]{2,1,0:T...) while((s32[]{:T(128)}, f32[192,4,2]{0,2,1:T(2,128)S(1)}, ...), condition=%wide.region_5.6_spmd.clone, body=%wide.region_2.5_spmd.clone.sunk | while | flops 623156736 | bytes 37257324 | solution.py:135
  130.3 2.6 constant_dynamic-slice_fusion.3
  132.9 1.4 copy.35
  134.3 6.0 bitcast_reduce_fusion.2
  140.4 5.4 fusion.51
  145.8 1.4 copy.36
  147.2 4.8 fusion.53
  152.1 2.6 constant_dynamic-slice_fusion.3
  154.7 1.4 copy.35
  156.1 6.0 bitcast_reduce_fusion.2
  162.1 5.4 fusion.51
  167.6 1.4 copy.36
  169.0 4.8 fusion.53
  173.9 1.5 convolution_convert_fusion.1
  176.0 1.4 copy.28
  177.4 5.4 stack.2
  182.8 5.0 all-to-all-start
  188.5 1.2 fusion.15
  189.9 2.5 all_gather.20
  192.5 338.7 %all-gather.9.cloned.1.call-done = bf16[2048,2816]{1,0:T(8,128)(2,1)} async-done(((bf16[128,2816]{1,0:T(8,128)(2,1)}), bf16[2048,2816]{1,0:T(8,128)(2,1)}) %all-gather.9.cloned.1.call-update) | async-done | bytes 11534352 | tf_op jit(solution)/shard_map/all_gather | solution.py:77
  531.1 8.1 %fusion.27 = f32[192,2816]{1,0:T(8,128)} fusion(bf16[192,2048]{1,0:T(8,128)(2,1)S(1)} %all_gather.20, bf16[2048,2816]{1,0:T(8,128)(2,1)} %all-gather.9.cloned.1.call-done), kind=kOutput, calls=%fused_computation.67 | convolution fusion | flops 2214592512 | bytes 14483456 | tf_op jit(solution)/shard_map/dot_general | solution.py:165
  539.2 140.7 %all-gather.11.cloned.1.call-done = bf16[2048,2816]{1,0:T(8,128)(2,1)} async-done(((bf16[128,2816]{1,0:T(8,128)(2,1)}), bf16[2048,2816]{1,0:T(8,128)(2,1)}) %all-gather.11.cloned.1.call-update) | async-done | bytes 11534352 | tf_op jit(solution)/shard_map/all_gather | solution.py:78
  679.9 15.2 %convolution_convert_fusion = bf16[192,2048]{1,0:T(8,128)(2,1)} fusion(bf16[2816,2048]{0,1:T(8,128)(2,1)} %bitcast.13, bf16[192,2048]{1,0:T(8,128)(2,1)S(1)} %all_gather.20, bf16[2048,2816]{1,0:T(8,128)(2,1)} %all-gather.11.cloned.1.call-done, f32[192,2816]{1,0:T(8,128)} %fusion.27), kind=kOutput, calls=%fused_computation.19 | convolution fusion | flops 4432822272 | bytes 26804224 | tf_op jit(solution)/shard_map/dot_general | solution.py:168
  695.2 6.5 reduce-scatter.5.cloned.1.call-done
  701.7 1.1 fusion.18
  702.8 2.4 all_gather.23
  705.1 0.9 copy.50
  (45 shorter events, 5.1 us)
Async XLA Ops:
  6.5 167.4 %copy-start = (bf16[512,2048]{1,0:T(8,128)(2,1)S(1)}, bf16[512,2048]{1,0:T(8,128)(2,1)}, u32[]{:S(2)}) copy-start(bf16[512,2048]{1,0:T(8,128)(2,1)} %param.18) | copy-start | bytes 6291460
  6.5 64.3 %all-gather.5.cloned.1.call-start = ((), (), s32[]{:S(2)}) async-start(), calls=%async_computation.3 | async-start | bytes 1671168 | tf_op jit(solution)/shard_map/all_gather | solution.py:146
  9.6 120.7 %all-gather.7.cloned.1.call-start = ((), (), s32[]{:S(2)}) async-start(), calls=%async_computation.4 | async-start | bytes 1671168 | tf_op jit(solution)/shard_map/all_gather | solution.py:147
  10.4 178.1 %reduce-scatter.3.cloned.1.call-start = ((), (), s32[]{:S(2)}) async-start(), calls=%async_computation.5 | async-start | bytes 1179648 | tf_op jit(solution)/shard_map/reduce_scatter | solution.py:152
  175.4 355.7 %all-gather.9.cloned.1.call-start = ((), (), s32[]{:S(2)}) async-start(), calls=%async_computation.6 | async-start | bytes 12255232 | tf_op jit(solution)/shard_map/all_gather | solution.py:77
  182.8 5.7 copy-start.1
  182.8 7.0 copy-start.2
  182.8 356.4 %all-to-all-start = ((bf16[16,2816,128]{1,2,0:T(8,128)(2,1)}), bf16[16,2816,128]{1,2,0:T(8,128)(2,1)}, u32[]{:S(2)}, u32[]{:S(2)}) async-start(bf16[16,2816,128]{1,2,0:T(8,128)(2,1)} %stack.2), calls=%async_computation.1 | async-start | bytes 23068672 | tf_op jit(solution)/shard_map/all_to_all | solution.py:79
  187.8 492.1 %all-gather.11.cloned.1.call-start = ((), (), s32[]{:S(2)}) async-start(), calls=%async_computation.7 | async-start | bytes 12255232 | tf_op jit(solution)/shard_map/all_gather | solution.py:78
  188.4 513.3 %reduce-scatter.5.cloned.1.call-start = ((), (), s32[]{:S(2)}) async-start(), calls=%async_computation.8 | async-start | bytes 1179648 | tf_op jit(solution)/shard_map/reduce_scatter | solution.py:169
Sparse Core Ops, SparseCore 0:
  10.1 60.6 all-gather.4
  73.6 56.6 all-gather.6
  175.5 6.8 reduce-scatter.2
  185.1 346.0 all-gather.8
  533.7 146.1 all-gather.10
  695.3 6.3 reduce-scatter.4
